TPU v7x, 768 devices: a whole 4x8x12 slice. The times are simulated.
768 devices in a mesh: row: 48 (over z, x), col: 16 (over y, core).
Axes of the slice: x: 4, y: 8, z: 12, core: 2. Of those that a mesh axis runs over, the one named last changes fastest.
Arguments:
- tokens: bfloat16 [6144, 4096], P('row'), may hold values from -6 to 6
- w_value: bfloat16 [2304, 4096], P('col'), may hold values from -0.09375 to 0.09375
- w_gate_one: bfloat16 [2304, 4096], P('col'), may hold values from -0.09375 to 0.09375
- w_gate_two: bfloat16 [2304, 4096], P('col'), may hold values from -0.09375 to 0.09375
- short_taps: float32 [3, 3, 2304], P(None, None, 'col'), may hold values from -3.5 to 3.5
- filter_in: float32 [33, 64], replicated, may hold values from -1 to 1
- filter_mid: float32 [64, 64], replicated, may hold values from -0.75 to 0.75
- filter_out: float32 [64, 2, 2, 2304], replicated, may hold values from -1 to 1
- decay_rate: float32 [2304], P('col'), may hold values from 0.5 to 49, as said below
- skip: float32 [2, 2304], P(None, 'col'), may hold values from -0.3 to 0.3
- w_out: bfloat16 [2304, 4096], P(None, 'col'), may hold values from -0.125 to 0.125
Outputs:
- mixed: bfloat16 [6144, 4096], P('row', 'col')
Inputs may be any that keep to these rules, and one draw needn't show every extreme that they name: `decay_rate`: each channel's rate is positive; per unit of the relative position t.
All inputs are finite; a program needn't handle non-finite values.
Results may differ from a plain program's by a relative error of at most 0.007.
Values may be sent and summed in bfloat16 or wider, within the bound.
A program may use at most 32 MiB of HBM per device.

v0:
```python
import math

import jax
import jax.numpy as jnp
from jax import lax
from jax.sharding import PartitionSpec as P

BANDS = 16


HIGHEST = lax.Precision.HIGHEST


def tables(row_count, col_count, modulus):
    product = (
        jnp.arange(row_count, dtype=jnp.int32)[:, None]
        * jnp.arange(col_count, dtype=jnp.int32)[None, :]
        % modulus
    )
    angles = product.astype(jnp.float32) * (2 * math.pi / modulus)
    return (jnp.cos(angles), jnp.sin(angles))


def forward_transform(signal, in_count, wide, block_len):
    leading = signal.shape[:-1]
    inner_b = min(block_len, 128)
    inner_a = block_len // inner_b
    shaped = signal.reshape(leading + (in_count, block_len))
    cos_one, sin_one = tables(wide, in_count, wide)
    real_part = jnp.einsum("kn,...nt->...kt", cos_one, shaped, precision=HIGHEST)
    imag_part = -jnp.einsum("kn,...nt->...kt", sin_one, shaped, precision=HIGHEST)
    cos_two, sin_two = tables(wide, block_len, wide * block_len)
    real_part, imag_part = (
        real_part * cos_two + imag_part * sin_two,
        imag_part * cos_two - real_part * sin_two,
    )
    real_part = real_part.reshape(leading + (wide, inner_a, inner_b))
    imag_part = imag_part.reshape(leading + (wide, inner_a, inner_b))
    cos_three, sin_three = tables(inner_a, inner_a, inner_a)
    real_part, imag_part = (
        jnp.einsum("ja,...kab->...kjb", cos_three, real_part, precision=HIGHEST)
        + jnp.einsum("ja,...kab->...kjb", sin_three, imag_part, precision=HIGHEST),
        jnp.einsum("ja,...kab->...kjb", cos_three, imag_part, precision=HIGHEST)
        - jnp.einsum("ja,...kab->...kjb", sin_three, real_part, precision=HIGHEST),
    )
    cos_four, sin_four = tables(inner_a, inner_b, block_len)
    real_part, imag_part = (
        real_part * cos_four + imag_part * sin_four,
        imag_part * cos_four - real_part * sin_four,
    )
    cos_five, sin_five = tables(inner_b, inner_b, inner_b)
    return (
        jnp.einsum("...jb,bm->...jm", real_part, cos_five, precision=HIGHEST)
        + jnp.einsum("...jb,bm->...jm", imag_part, sin_five, precision=HIGHEST),
        jnp.einsum("...jb,bm->...jm", imag_part, cos_five, precision=HIGHEST)
        - jnp.einsum("...jb,bm->...jm", real_part, sin_five, precision=HIGHEST),
    )


def inverse_transform(real_part, imag_part, out_count, wide, block_len):
    leading = real_part.shape[:-3]
    inner_b = min(block_len, 128)
    inner_a = block_len // inner_b
    cos_five, sin_five = tables(inner_b, inner_b, inner_b)
    real_part, imag_part = (
        jnp.einsum("...jm,mb->...jb", real_part, cos_five, precision=HIGHEST)
        - jnp.einsum("...jm,mb->...jb", imag_part, sin_five, precision=HIGHEST),
        jnp.einsum("...jm,mb->...jb", imag_part, cos_five, precision=HIGHEST)
        + jnp.einsum("...jm,mb->...jb", real_part, sin_five, precision=HIGHEST),
    )
    cos_four, sin_four = tables(inner_a, inner_b, block_len)
    real_part, imag_part = (
        real_part * cos_four - imag_part * sin_four,
        imag_part * cos_four + real_part * sin_four,
    )
    cos_three, sin_three = tables(inner_a, inner_a, inner_a)
    real_part, imag_part = (
        jnp.einsum("aj,...kjb->...kab", cos_three, real_part, precision=HIGHEST)
        - jnp.einsum("aj,...kjb->...kab", sin_three, imag_part, precision=HIGHEST),
        jnp.einsum("aj,...kjb->...kab", cos_three, imag_part, precision=HIGHEST)
        + jnp.einsum("aj,...kjb->...kab", sin_three, real_part, precision=HIGHEST),
    )
    real_part = real_part.reshape(leading + (wide, block_len))
    imag_part = imag_part.reshape(leading + (wide, block_len))
    cos_two, sin_two = tables(wide, block_len, wide * block_len)
    real_part, imag_part = (
        real_part * cos_two - imag_part * sin_two,
        imag_part * cos_two + real_part * sin_two,
    )
    cos_one, sin_one = tables(out_count, wide, wide)
    result = jnp.einsum("nk,...kt->...nt", cos_one, real_part, precision=HIGHEST) - jnp.einsum(
        "nk,...kt->...nt", sin_one, imag_part, precision=HIGHEST
    )
    return (result / (wide * block_len)).reshape(leading + (out_count * block_len,))


def short_filter(padded, filter_taps):
    return (
        padded[..., :-2] * filter_taps[:, 0, :, None]
        + padded[..., 1:-1] * filter_taps[:, 1, :, None]
        + padded[..., 2:] * filter_taps[:, 2, :, None]
    )


def filter_bank(seq_len, filter_in, filter_mid, out_block, rate_block):
    positions = jnp.arange(seq_len, dtype=jnp.float32)
    relative = positions / (seq_len - 1)
    bands = jnp.linspace(0.0001, BANDS - 1, BANDS, dtype=jnp.float32)
    angles = 2 * math.pi / seq_len * positions[:, None] * bands[None, :]
    feats = jnp.concatenate([relative[:, None], jnp.cos(angles), jnp.sin(angles)], axis=1)
    hidden = jnp.sin(jnp.dot(feats, filter_in, precision=HIGHEST))
    hidden = jnp.sin(jnp.dot(hidden, filter_mid, precision=HIGHEST))
    filter_taps = jnp.einsum("lh,hodc->odcl", hidden, out_block, precision=HIGHEST)
    decay = jnp.exp(-relative[None, :] * rate_block[:, None])
    return filter_taps * decay


def on_device(
    tokens,
    w_value,
    w_gate_one,
    w_gate_two,
    short_taps,
    filter_in,
    filter_mid,
    filter_out,
    decay_rate,
    skip,
    w_out,
):
    n_rows = lax.axis_size("row")
    row_index = lax.axis_index("row")
    col_index = lax.axis_index("col")
    local_width = w_value.shape[0]
    chan_dev = local_width // n_rows
    projected = jnp.stack(
        [
            jnp.einsum("td,cd->ct", tokens, weight, preferred_element_type=jnp.float32)
            for weight in (w_value, w_gate_one, w_gate_two)
        ]
    ).astype(jnp.bfloat16)
    block_len = projected.shape[2]
    seq_len = n_rows * block_len
    wide = 2 * n_rows
    moved = lax.all_to_all(projected, "row", split_axis=1, concat_axis=2, tiled=True)
    own_taps = lax.dynamic_slice_in_dim(short_taps, row_index * chan_dev, chan_dev, 2)
    bordered = jnp.pad(moved.astype(jnp.float32), ((0, 0), (0, 0), (1, 1)))
    channel_major = short_filter(bordered, own_taps)
    global_start = col_index * local_width + row_index * chan_dev
    own_out = lax.dynamic_slice_in_dim(filter_out, global_start, chan_dev, 3)
    own_rate = lax.dynamic_slice_in_dim(decay_rate, row_index * chan_dev, chan_dev, 0)
    own_skip = lax.dynamic_slice_in_dim(skip, row_index * chan_dev, chan_dev, 1)
    filter_taps = filter_bank(seq_len, filter_in, filter_mid, own_out, own_rate)
    forward_part = filter_taps[:, 0]
    backward_part = filter_taps[:, 1]
    kern = jnp.concatenate(
        [
            forward_part,
            jnp.zeros(forward_part[..., :1].shape, jnp.float32),
            backward_part[..., 1:][..., ::-1],
        ],
        axis=-1,
    )
    kern_real, kern_imag = forward_transform(kern, wide, wide, block_len)
    signal = channel_major[0]
    for order_index in range(2):
        sig_real, sig_imag = forward_transform(signal, n_rows, wide, block_len)
        prod_real = sig_real * kern_real[order_index] - sig_imag * kern_imag[order_index]
        prod_imag = sig_real * kern_imag[order_index] + sig_imag * kern_real[order_index]
        long_part = inverse_transform(prod_real, prod_imag, n_rows, wide, block_len)
        signal = channel_major[order_index + 1] * (
            long_part + own_skip[order_index][:, None] * signal
        )
    mixer_channels = signal.astype(jnp.bfloat16)
    position_major = lax.all_to_all(mixer_channels, "row", split_axis=1, concat_axis=0, tiled=True)
    totals = jnp.einsum(
        "ct,cd->td",
        lax.all_gather(position_major, "col", axis=0, tiled=True),
        w_out,
        preferred_element_type=jnp.float32,
    )
    return totals.astype(jnp.bfloat16)


def solution(mesh):
    placed = (
        P("row", None),
        P("col", None),
        P("col", None),
        P("col", None),
        P(None, None, "col"),
        P(),
        P(),
        P(),
        P("col"),
        P(None, "col"),
        P(None, "col"),
    )
    return jax.shard_map(
        on_device, mesh=mesh, in_specs=placed, out_specs=P("row", "col"), check_vma=False
    )
```

profile of v0, /device:TPU:1, one launch (start us, length us, event | category | flops | bytes accessed | tf_op | source)
XLA Modules:
  0.0 115.6 jit_solution(17897224620988180023)
XLA Ops:
  0.0 2.2 %fusion.13 = bf16[1,144,128]{2,1,0:T(8,128)(2,1)S(1)} fusion(bf16[144,4096]{1,0:T(8,128)(2,1)} %param.12, bf16[128,4096]{1,0:T(8,128)(2,1)} %param.11), kind=kOutput, calls=%fused_computation.38 | convolution fusion | flops 151013376 | bytes 2265088 | tf_op jit(solution)/shard_map/td,cd->ct/dot_general | solution.py:138
  2.9 0.8 copy-done.4
  4.2 0.7 copy.25
  4.9 18.8 %all-to-all-start = ((bf16[3,144,128]{2,0,1:T(4,128)(2,1)}), bf16[3,144,128]{2,0,1:T(4,128)(2,1)S(1)}, u32[]{:S(2)}, u32[]{:S(2)}) async-start(bf16[3,144,128]{2,0,1:T(4,128)(2,1)} %copy.25), calls=%async_computation | async-start | bytes 294912 | tf_op jit(solution)/shard_map/all_to_all | solution.py:145
  24.4 1.4 %multiply_cosine_fusion = (f32[6144,16]{0,1:T(8,128)S(1)}, f32[6144,16]{0,1:T(8,128)S(1)}) fusion(f32[16]{0:T(128)S(1)} %pad_maximum_fusion.1, f32[6144]{0:T(1024)S(1)} %iota_multiply_fusion), kind=kLoop, calls=%fused_computation.47 | loop fusion | flops 98304 | bytes 811072 | tf_op jit(solution)/shard_map/cos | solution.py:110
  25.8 8.0 %convolution_sine_fusion = f32[6144,64]{0,1:T(8,128)S(1)} fusion(f32[33,64]{1,0:T(8,128)S(1)} %copy-done.6, f32[6144,16]{0,1:T(8,128)S(1)} %get-tuple-element.19, f32[6144,16]{0,1:T(8,128)S(1)} %get-tuple-element.18, f32[6144,1]{0,1:T(1,128)S(1)} %iota_multiply_fusion.1), kind=kOutput, calls=%fused_computation | convolution fusion | flops 156119040 | bytes 2392320 | tf_op jit(solution)/shard_map/dot_general | solution.py:111
  33.8 8.0 %fusion = f32[6144,64,1,1]{0,1,3,2:T(8,128)S(1)} fusion(f32[6144,64]{0,1:T(8,128)S(1)} %convolution_sine_fusion, f32[64,64]{1,0:T(8,128)S(1)} %copy-done.5), kind=kOutput, calls=%fused_computation.2 | convolution fusion | flops 301989888 | bytes 3162112 | tf_op jit(solution)/shard_map/dot_general | solution.py:112
  41.8 0.9 convolution_multiply_fusion
  43.0 4.4 %reverse = f32[2,3,6144]{2,1,0:T(4,128)S(1)} reverse(f32[2,3,6144]{2,1,0:T(4,128)S(1)} %bitcast.214), dimensions={2} | reverse | bytes 294912
  48.2 0.6 convolution_bitcast_fusion
  48.8 0.6 fusion.1
  49.7 0.7 fusion.51
  50.4 1.4 %fusion.53 = f32[2,3,96,128]{3,2,1,0:T(8,128)} fusion(f32[2,3,96,128]{3,2,1,0:T(8,128)S(1)} %fusion.1, f32[96,128]{1,0:T(8,128)S(1)} %get-tuple-element.27, f32[2,3,96,128]{3,2,1,0:T(8,128)S(1)} %convolution_bitcast_fusion, f32[96,128]{1,0:T(8,128)S(1)} %get-tuple-element.28), kind=kOutput, calls=%fused_computation.129 | convolution fusion | flops 114360320 | bytes 983040 | tf_op jit(solution)/shard_map/...jb,bm->...jm/dot_general | solution.py:53
  51.8 0.7 convolution_subtract_fusion
  52.6 0.9 constant_dynamic-slice_fusion.1
  53.6 2.4 %convolution_add_fusion = f32[2,3,96,128]{3,2,1,0:T(8,128)} fusion(f32[2,3,96,128]{3,2,1,0:T(8,128)} %fusion.53, f32[2,3,96,128]{3,2,1,0:T(8,128)S(1)} %fusion.1, f32[96,128]{1,0:T(8,128)S(1)} %get-tuple-element.27, f32[2,3,96,128]{3,2,1,0:T(8,128)S(1)} %convolution_bitcast_fusion, f32[96,128]{1,0:T(8,128)S(1)} %get-tuple-element.28), kind=kOutput, calls=%fused_computation.5 | convolution fusion | flops 114434048 | bytes 1277952 | tf_op jit(solution)/shard_map/...jb,bm->...jm/dot_general | solution.py:54
  58.5 0.5 convolution_add_fusion.4
  59.0 0.6 multiply_add_fusion.12
  64.0 0.7 fusion.69
  64.7 0.5 convolution_add_fusion.2
  65.3 0.6 multiply_add_fusion.6
  68.8 22.8 %all_to_all.25 = bf16[3,48,128]{2,0,1:T(4,128)(2,1)S(1)} all-to-all(bf16[3,48,128]{2,0,1:T(4,128)(2,1)S(1)} %copy.31), channel_id=1, replica_groups=mesh['row'=48,'col'=16] {'row'}, dimensions={1} | all-to-all | bytes 73728 | tf_op jit(solution)/shard_map/all_to_all | solution.py:175
  91.6 21.7 %all_gather.3 = bf16[2304,128]{1,0:T(8,128)(2,1)S(1)} all-gather(bf16[144,128]{1,0:T(8,128)(2,1)S(1)} %all_to_all.22), channel_id=1, replica_groups=mesh['row'=48,'col'=16] {'col'}, dimensions={0}, use_global_device_ids=true | all-gather | bytes 626688 | tf_op jit(solution)/shard_map/all_gather | solution.py:178
  113.3 2.3 %convolution_convert_fusion = bf16[128,256]{1,0:T(8,128)(2,1)} fusion(bf16[2304,128]{1,0:T(8,128)(2,1)S(1)} %all_gather.3, bf16[2304,256]{1,0:T(8,128)(2,1)} %param.21), kind=kOutput, calls=%fused_computation.23 | convolution fusion | flops 151027712 | bytes 1835008 | tf_op jit(solution)/shard_map/ct,cd->td/dot_general | solution.py:176
  (65 shorter events, 12.7 us)
Async XLA Ops:
  0.0 23.9 %copy-start = (f32[64,2,2,2304]{3,2,1,0:T(2,128)S(1)}, f32[64,2,2,2304]{3,2,1,0:T(2,128)}, u32[]{:S(2)}) copy-start(f32[64,2,2,2304]{3,2,1,0:T(2,128)} %param.18) | copy-start | bytes 7077892
  0.0 2.2 %copy-start.1 = (bf16[128,4096]{1,0:T(8,128)(2,1)S(1)}, bf16[128,4096]{1,0:T(8,128)(2,1)}, u32[]{:S(2)}) copy-start(bf16[128,4096]{1,0:T(8,128)(2,1)} %param.11) | copy-start | bytes 3145732
  0.0 2.4 %copy-start.3 = (bf16[144,4096]{1,0:T(8,128)(2,1)S(1)}, bf16[144,4096]{1,0:T(8,128)(2,1)}, u32[]{:S(2)}) copy-start(bf16[144,4096]{1,0:T(8,128)(2,1)} %param.13) | copy-start | bytes 3538948
  2.4 1.3 %copy-start.4 = (bf16[144,4096]{1,0:T(8,128)(2,1)S(1)}, bf16[144,4096]{1,0:T(8,128)(2,1)}, u32[]{:S(2)}) copy-start(bf16[144,4096]{1,0:T(8,128)(2,1)} %param.14) | copy-start | bytes 3538948
  3.7 20.4 %copy-start.8 = (f32[144]{0:T(256)S(1)}, f32[144]{0:T(256)}, u32[]{:S(2)}) copy-start(f32[144]{0:T(256)} %param.19) | copy-start | bytes 1732
  4.2 21.7 %copy-start.6 = (f32[33,64]{1,0:T(8,128)S(1)}, f32[33,64]{1,0:T(8,128)}, u32[]{:S(2)}) copy-start(f32[33,64]{1,0:T(8,128)} %param.16) | copy-start | bytes 25348
  4.9 51.0 %all-to-all-start = ((bf16[3,144,128]{2,0,1:T(4,128)(2,1)}), bf16[3,144,128]{2,0,1:T(4,128)(2,1)S(1)}, u32[]{:S(2)}, u32[]{:S(2)}) async-start(bf16[3,144,128]{2,0,1:T(4,128)(2,1)} %copy.25), calls=%async_computation | async-start | bytes 294912 | tf_op jit(solution)/shard_map/all_to_all | solution.py:145
  25.8 8.0 %copy-start.5 = (f32[64,64]{1,0:T(8,128)S(1)}, f32[64,64]{1,0:T(8,128)}, u32[]{:S(2)}) copy-start(f32[64,64]{1,0:T(8,128)} %param.17) | copy-start | bytes 49156
  50.4 2.2 %copy-start.7 = (f32[2,144]{1,0:T(2,128)S(1)}, f32[2,144]{1,0:T(2,128)}, u32[]{:S(2)}) copy-start(f32[2,144]{1,0:T(2,128)} %param.20) | copy-start | bytes 3460
  56.5 2.5 %copy-start.2 = (f32[2,3,96,128]{3,2,1,0:T(8,128)S(1)}, f32[2,3,96,128]{3,2,1,0:T(8,128)}, u32[]{:S(2)}) copy-start(f32[2,3,96,128]{3,2,1,0:T(8,128)} %convolution_add_fusion) | copy-start | bytes 884740
where the time goes:
time: 116 us
  blocking collectives  44.5 us (38%)
  matrix products  40.8 us (35%)
  starting transfers between devices  18.8 us (16%)
  local copies, waits for them, and re-layouts  8.61 us (7%)
  other arithmetic  2.34 us (2%)
    all_to_all x1, blocking collectives, on_device(): lax.all_to_all(mixer_channels, 'row', split_axis=1, concat_axis=0, tiled=...  22.8 us
    all_gather x1, blocking collectives, on_device(): lax.all_gather(position_major, 'col', axis=0, tiled=True)  21.7 us
    all_to_all x1, starting transfers between devices, on_device(): lax.all_to_all(projected, 'row', split_axis=1, concat_axis=2, tiled=True)  18.8 us
    dot_general x1, matrix products, filter_bank(): hidden = jnp.sin(jnp.dot(feats, filter_in, precision=HIGHEST))  7.98 us
    dot_general x1, matrix products, filter_bank(): hidden = jnp.sin(jnp.dot(hidden, filter_mid, precision=HIGHEST))  7.98 us
    unnamed x23, local copies, waits for them, and re-layouts  5.67 us
    dot_general x3, matrix products, forward_transform(): jnp.einsum('...jb,bm->...jm', imag_part, sin_five, precision=HIGHEST)  3.45 us
    dot_general x3, matrix products, on_device(): jnp.einsum('td,cd->ct', tokens, weight, preferred_element_type=jnp.float32)  3.14 us
  transfers between devices with their start and end apart: 1, of which 0 were waited for; matrix products, arithmetic and copies ran while one was open for 28% of the time, Pallas kernels for 0%

commit v1 on v0

v1 whole, which is shorter than its diff:
```python
import functools
import math

import jax
import jax.numpy as jnp
import ml_dtypes
import numpy as np
from jax import lax
from jax.experimental import pallas as pl
from jax.experimental.pallas import tpu as pltpu
from jax.sharding import PartitionSpec as P

BANDS = 16
BLOCK = 128
CHUNK_BLOCKS = 4
SINE = (
    6.283185272722434,
    -41.34169706895579,
    81.60502462256538,
    -76.70155117606154,
    42.01616582018448,
    -14.868610989100207,
    3.199693650180954,
)
MESH = pl.DeviceIdType.MESH
F32 = jnp.float32
BF16 = jnp.bfloat16


def halves(table):
    high = table.astype(ml_dtypes.bfloat16)
    low = (table - high.astype(np.float64)).astype(ml_dtypes.bfloat16)
    return high, low


def constants(rows, seq_len):
    wide = 2 * rows
    total = wide * BLOCK
    odd = np.arange(rows)[:, None] + 0.5
    blocks = np.arange(rows)[None, :]
    one = 2 * np.pi * odd * blocks / wide
    first = np.concatenate([np.cos(one), -np.sin(one)], axis=0)
    last = np.concatenate([np.cos(one).T, -np.sin(one).T], axis=1) * (2.0 / total)
    first_h, first_l = halves(first)
    last_h, last_l = halves(last)
    first = np.concatenate([first_h, first_l, first_h], axis=1)
    last = np.concatenate([last_h, last_l, last_h], axis=1)
    lanes = np.arange(BLOCK)
    two = 2 * np.pi * odd * lanes[None, :] / total
    twiddle = np.stack([np.cos(two), np.sin(two)]).astype(np.float32)
    three = 2 * np.pi * (lanes[:, None] * lanes[None, :] % BLOCK) / BLOCK
    cosine, sine = np.cos(three), np.sin(three)
    forward = np.block([[cosine, -sine], [sine, cosine]])
    inverse = np.block([[cosine, sine], [-sine, cosine]])
    square = np.stack([*halves(forward), *halves(inverse)])
    chunk = CHUNK_BLOCKS * BLOCK
    bands = np.linspace(0.0001, BANDS - 1, BANDS, dtype=np.float32).astype(np.float64)
    rate = 2 * np.pi / seq_len * bands[:, None]
    inside = rate * np.arange(chunk)[None, :]
    base = np.concatenate([np.cos(inside), np.sin(inside)]).astype(np.float32)
    steps = np.arange(seq_len // chunk)[:, None, None] * chunk * rate[None]
    turn = np.concatenate([np.cos(steps), np.sin(steps)], axis=1)
    turn = np.broadcast_to(turn, turn.shape[:2] + (BLOCK,)).astype(np.float32)
    return first, last, twiddle, square, base, np.ascontiguousarray(turn)


def dot(left, right, dims=((1,), (0,))):
    return lax.dot_general(left, right, (dims, ((), ())), preferred_element_type=F32)


def split(value):
    high = value.astype(BF16)
    return high, (value - high.astype(F32)).astype(BF16)


def sine_of_turns(turns):
    part = turns - jnp.round(turns)
    square = part * part
    total = jnp.full_like(square, SINE[-1])
    for coefficient in SINE[-2::-1]:
        total = total * square + coefficient
    return total * part


def stacked(value):
    high, low = split(value)
    return jnp.concatenate([high, high, low], axis=0)


def tripled(weights, width):
    high = weights.astype(BF16).astype(F32)
    lane = lax.broadcasted_iota(jnp.int32, weights.shape, 1)
    middle = (lane >= width) & (lane < 2 * width)
    return jnp.where(middle, weights - high, high).astype(BF16)


def kernel(
    sizes,
    taps_s,
    skip_s,
    rate_s,
    tokens_h,
    value_h,
    gate_one_h,
    gate_two_h,
    out_h,
    params,
    first,
    last,
    twiddle,
    square,
    base,
    turn,
    result,
    tokens_v,
    weights_v,
    out_v,
    plain,
    spread,
    gathered_taps,
    spectra,
    send_v,
    send_g,
    recv_v,
    recv_g,
    send_y,
    recv_y,
    blocks,
    load_sem,
    send_sem,
    recv_sem,
    near_send,
    near_recv,
    pair_send,
    pair_recv,
):
    rows, cols, chan, early = sizes
    width = rows * chan
    chips = cols // 2
    row = lax.axis_index("row")
    col = lax.axis_index("col")
    place = col // 2
    core = col % 2
    partner = place * 2 + 1 - core

    loads = [
        pltpu.make_async_copy(tokens_h, tokens_v, load_sem.at[0]),
        pltpu.make_async_copy(value_h, weights_v.at[0], load_sem.at[1]),
        pltpu.make_async_copy(gate_one_h, weights_v.at[1], load_sem.at[2]),
        pltpu.make_async_copy(gate_two_h, weights_v.at[2], load_sem.at[3]),
        pltpu.make_async_copy(out_h, out_v, load_sem.at[4]),
    ]
    for load in loads:
        load.start()

    barrier = pltpu.get_barrier_semaphore()

    @pl.loop(1, rows)
    def _(step):
        other = lax.rem(row + step, rows)
        pl.semaphore_signal(barrier, inc=1, device_id=(other, col), device_id_type=MESH)

    @pl.loop(1, chips)
    def _(step):
        other = lax.rem(place + step, chips) * 2 + core
        pl.semaphore_signal(barrier, inc=1, device_id=(row, other), device_id_type=MESH)

    pl.semaphore_signal(barrier, inc=1, device_id=(row, partner), device_id_type=MESH)

    loads[0].wait()
    for which in range(3):
        loads[1 + which].wait()
        projected = dot(weights_v[which], tokens_v[...], ((1,), (1,)))
        plain[...] = projected.astype(BF16).astype(F32)
        stride, offset = (4, 0) if which == 0 else (8, (which - 1) * chan)
        for q in range(chan):
            spread[pl.ds(offset + q, rows, stride=stride), :] = plain[
                pl.ds(q, rows, stride=chan), :
            ]
        if which == 0:
            for q in range(chan, 4):
                spread[pl.ds(q, rows, stride=4), :] = jnp.zeros((rows, BLOCK), F32)
            for r in range(rows):
                send_v[r] = spread[4 * r : 4 * r + 4, :].astype(BF16)
    for q in range(2 * chan, 8):
        spread[pl.ds(q, rows, stride=8), :] = jnp.zeros((rows, BLOCK), F32)
    for r in range(rows):
        send_g[r] = spread[8 * r : 8 * r + 8, :].astype(BF16)

    n_chunks = rows // CHUNK_BLOCKS
    chunk = CHUNK_BLOCKS * BLOCK
    seq_len = rows * BLOCK
    in_w = tripled(params[0:64, 0:144], 48)
    mid_w = tripled(params[64:128, 0:192], 64)
    out_w = tripled(params[128:144, 0:192], 64)
    rate_rows = jnp.zeros((16, BLOCK), F32)
    channel = lax.rem(lax.broadcasted_iota(jnp.int32, (16, BLOCK), 0), chan)
    for q in range(chan):
        rate_rows = jnp.where(channel == q, rate_s[row * chan + q], rate_rows)
    rate_rows = jnp.concatenate([rate_rows] * CHUNK_BLOCKS, axis=1)

    def filter_chunk(index):
        lane = lax.broadcasted_iota(jnp.int32, (16, chunk), 1)
        relative = (lane + index * chunk).astype(F32) * (1.0 / (seq_len - 1))
        first_row = lax.broadcasted_iota(jnp.int32, (16, chunk), 0) == 0
        turn_c = jnp.concatenate([turn[index, 0:BANDS, :]] * CHUNK_BLOCKS, axis=1)
        turn_s = jnp.concatenate([turn[index, BANDS : 2 * BANDS, :]] * CHUNK_BLOCKS, axis=1)
        base_c, base_s = base[0:BANDS, :], base[BANDS : 2 * BANDS, :]
        feats = jnp.concatenate(
            [
                base_c * turn_c - base_s * turn_s,
                base_s * turn_c + base_c * turn_s,
                jnp.where(first_row, relative, 0.0),
            ],
            axis=0,
        )
        hidden = sine_of_turns(dot(in_w, stacked(feats)))
        hidden = sine_of_turns(dot(mid_w, stacked(hidden)))
        filter_taps = dot(out_w, stacked(hidden)) * jnp.exp(-relative * rate_rows)
        for b in range(CHUNK_BLOCKS):
            start = pl.multiple_of((index * CHUNK_BLOCKS + b) * 16, 16)
            gathered_taps[pl.ds(start, 16), :] = filter_taps[:, b * BLOCK : (b + 1) * BLOCK]

    @pl.loop(0, early)
    def _(index):
        filter_chunk(index)

    pl.semaphore_wait(barrier, rows - 1 + chips - 1 + 1)

    def send(source, landing, which, order):
        @pl.loop(0, rows - 1)
        def _(step):
            half = (step + 1) // 2
            sign = 1 - 2 * lax.rem(step, 2)
            other = lax.rem(row + rows // 2 + rows + sign * half, rows)
            pltpu.make_async_remote_copy(
                src_ref=source.at[other],
                dst_ref=landing.at[row],
                send_sem=send_sem.at[which],
                recv_sem=recv_sem.at[which],
                device_id=(other, col),
                device_id_type=MESH,
            ).start()

    def all_of(source, landing, which):
        return pltpu.make_async_remote_copy(
            src_ref=source.at[pl.ds(0, rows - 1)],
            dst_ref=landing.at[pl.ds(0, rows - 1)],
            send_sem=send_sem.at[which],
            recv_sem=recv_sem.at[which],
            device_id=(lax.rem(row + 1, rows), col),
            device_id_type=MESH,
        )

    send(send_v, recv_v, 0, 0)
    send(send_g, recv_g, 1, 0)
    recv_v[row] = send_v[row]
    recv_g[row] = send_g[row]

    @pl.loop(early, n_chunks)
    def _(index):
        filter_chunk(index)

    tw_c, tw_s = twiddle[0], twiddle[1]

    def forward(signals):
        reals, imags = [], []
        for signal in signals:
            both = dot(first[...], stacked(signal))
            re, im = both[:rows], both[rows:]
            reals.append(re * tw_c + im * tw_s)
            imags.append(im * tw_c - re * tw_s)
        both = jnp.concatenate(
            [jnp.concatenate(reals, axis=0), jnp.concatenate(imags, axis=0)], axis=1
        )
        high, low = split(both)
        return dot(high, square[0]) + dot(high, square[1]) + dot(low, square[0])

    def backward(spectrum):
        high, low = split(spectrum)
        both = dot(high, square[2]) + dot(high, square[3]) + dot(low, square[2])
        signals = []
        for q in range(chan):
            re = both[q * rows : (q + 1) * rows, :BLOCK]
            im = both[q * rows : (q + 1) * rows, BLOCK:]
            turned = jnp.concatenate([re * tw_c - im * tw_s, im * tw_c + re * tw_s], axis=0)
            signals.append(dot(last[...], stacked(turned)))
        return signals

    lane = lax.broadcasted_iota(jnp.int32, (rows, BLOCK), 1)
    line = lax.broadcasted_iota(jnp.int32, (rows, BLOCK), 0)
    origin = (lane == 0) & (line == 0)
    for order in range(2):
        ahead, behind = [], []
        for q in range(chan):
            base_row = (order * 2) * chan + q
            ahead.append(gathered_taps[pl.ds(base_row, rows, stride=16), :])
            back = gathered_taps[pl.ds(base_row + chan, rows, stride=16), :]
            behind.append(jnp.where(origin, 0.0, back))
        ahead = forward(ahead)
        behind = forward(behind)
        spectra[order, :, :BLOCK] = ahead[:, :BLOCK] + behind[:, :BLOCK]
        spectra[order, :, BLOCK:] = ahead[:, BLOCK:] - behind[:, BLOCK:]

    def short(signal, which, q):
        before = pltpu.roll(signal, 1, 1)
        before = jnp.where(lane == 0, pltpu.roll(before, 1, 0), before)
        before = jnp.where(origin, 0.0, before)
        after = pltpu.roll(signal, BLOCK - 1, 1)
        after = jnp.where(lane == BLOCK - 1, pltpu.roll(after, rows - 1, 0), after)
        after = jnp.where((lane == BLOCK - 1) & (line == rows - 1), 0.0, after)
        at = row * chan + q
        return (
            before * taps_s[which * 3, at]
            + signal * taps_s[which * 3 + 1, at]
            + after * taps_s[which * 3 + 2, at]
        )

    all_of(send_v, recv_v, 0).wait_recv()
    for r in range(rows):
        spread[4 * r : 4 * r + 4, :] = recv_v[r].astype(F32)
    signals = [short(spread[pl.ds(q, rows, stride=4), :], 0, q) for q in range(chan)]

    for order in range(2):
        spectrum = forward(signals)
        re, im = spectrum[:, :BLOCK], spectrum[:, BLOCK:]
        kern_re, kern_im = spectra[order, :, :BLOCK], spectra[order, :, BLOCK:]
        product = jnp.concatenate(
            [re * kern_re - im * kern_im, re * kern_im + im * kern_re], axis=1
        )
        longs = backward(product)
        if order == 0:
            all_of(send_g, recv_g, 1).wait_recv()
            for r in range(rows):
                spread[8 * r : 8 * r + 8, :] = recv_g[r].astype(F32)
        for q in range(chan):
            gate = short(spread[pl.ds(order * chan + q, rows, stride=8), :], 1 + order, q)
            signals[q] = gate * (longs[q] + skip_s[order, row * chan + q] * signals[q])

    for q in range(4):
        spread[pl.ds(q, rows, stride=4), :] = (
            signals[q] if q < chan else jnp.zeros((rows, BLOCK), F32)
        )
    for r in range(rows):
        send_y[r] = spread[4 * r : 4 * r + 4, :].astype(BF16)
    send(send_y, recv_y, 2, 0)
    recv_y[row] = send_y[row]
    all_of(send_y, recv_y, 2).wait_recv()
    for r in range(rows):
        spread[4 * r : 4 * r + 4, :] = recv_y[r].astype(F32)
    for q in range(chan):
        plain[pl.ds(q, rows, stride=chan), :] = spread[pl.ds(q, rows, stride=4), :]
    blocks[col] = plain[...].astype(BF16)

    def to_chip(step):
        return pltpu.make_async_remote_copy(
            src_ref=blocks.at[col],
            dst_ref=blocks.at[col],
            send_sem=near_send.at[step],
            recv_sem=near_recv.at[step],
            device_id=(row, lax.rem(place + step, chips) * 2 + core),
            device_id_type=MESH,
        )

    def to_pair(step):
        own = lax.rem(place + chips - step, chips) * 2 + core
        return pltpu.make_async_remote_copy(
            src_ref=blocks.at[own],
            dst_ref=blocks.at[own],
            send_sem=pair_send.at[step],
            recv_sem=pair_recv.at[step],
            device_id=(row, partner),
            device_id_type=MESH,
        )

    def block_product(index):
        start = pl.multiple_of(index * width, 16)
        return dot(blocks[index], out_v[pl.ds(start, width), :], ((0,), (0,)))

    near_first = [s for d in range(1, chips // 2 + 1) for s in sorted({d, chips - d})]
    for step in near_first[::-1]:
        to_chip(step).start()
    to_pair(0).start()
    loads[4].wait()
    total = block_product(col)
    for step in near_first:
        to_chip(step).wait_recv()
        to_pair(step).start()
        total += block_product(lax.rem(place + chips - step, chips) * 2 + core)
    for step in [0] + near_first:
        to_pair(step).wait_recv()
        total += block_product(lax.rem(place + chips - step, chips) * 2 + 1 - core)
    result[...] = total.astype(BF16)

    for source, landing, which in ((send_v, recv_v, 0), (send_g, recv_g, 1), (send_y, recv_y, 2)):
        all_of(source, landing, which).wait_send()
    for step in near_first:
        to_chip(step).wait_send()
    for step in [0] + near_first:
        to_pair(step).wait_send()


def on_device(
    tokens,
    w_value,
    w_gate_one,
    w_gate_two,
    short_taps,
    filter_in,
    filter_mid,
    filter_out,
    decay_rate,
    skip,
    w_out,
):
    rows, cols = lax.axis_size("row"), lax.axis_size("col")
    row, col = lax.axis_index("row"), lax.axis_index("col")
    width, depth = w_value.shape
    chan = width // rows
    seq_len = rows * BLOCK
    own_out = lax.dynamic_slice_in_dim(filter_out, col * width + row * chan, chan, 3)
    turns = 1 / (2 * math.pi)
    first_w = jnp.concatenate([filter_in[1:], filter_in[:1]]).T * turns
    first_w = jnp.pad(first_w, ((0, 0), (0, 48 - first_w.shape[1])))
    last_w = jnp.pad(own_out.reshape(64, 4 * chan).T, ((0, 16 - 4 * chan), (0, 0)))
    params = jnp.concatenate(
        [
            jnp.pad(jnp.tile(first_w, (1, 3)), ((0, 0), (0, 112))),
            jnp.pad(jnp.tile(filter_mid.T * turns, (1, 3)), ((0, 0), (0, 64))),
            jnp.pad(jnp.tile(last_w, (1, 3)), ((0, 0), (0, 64))),
        ]
    )
    tables = [jnp.asarray(table) for table in constants(rows, seq_len)]
    smem = pl.BlockSpec(memory_space=pltpu.SMEM)
    vmem = pl.BlockSpec(memory_space=pltpu.VMEM)
    hbm = pl.BlockSpec(memory_space=pl.ANY)
    early = min(EARLY, rows // CHUNK_BLOCKS)
    return pl.pallas_call(
        functools.partial(kernel, (rows, cols, chan, early)),
        out_shape=jax.ShapeDtypeStruct((BLOCK, w_out.shape[1]), BF16),
        in_specs=[smem] * 3 + [hbm] * 5 + [vmem] * 7,
        out_specs=vmem,
        scratch_shapes=[
            pltpu.VMEM((BLOCK, depth), BF16),
            pltpu.VMEM((3, width, depth), BF16),
            pltpu.VMEM(w_out.shape, BF16),
            pltpu.VMEM((width, BLOCK), F32),
            pltpu.VMEM((8 * rows, BLOCK), F32),
            pltpu.VMEM((16 * rows, BLOCK), F32),
            pltpu.VMEM((2, width, 2 * BLOCK), F32),
            pltpu.VMEM((rows, 4, BLOCK), BF16),
            pltpu.VMEM((rows, 8, BLOCK), BF16),
            pltpu.VMEM((rows, 4, BLOCK), BF16),
            pltpu.VMEM((rows, 8, BLOCK), BF16),
            pltpu.VMEM((rows, 4, BLOCK), BF16),
            pltpu.VMEM((rows, 4, BLOCK), BF16),
            pltpu.VMEM((cols, width, BLOCK), BF16),
            pltpu.SemaphoreType.DMA((5,)),
            pltpu.SemaphoreType.DMA((3,)),
            pltpu.SemaphoreType.DMA((3,)),
            pltpu.SemaphoreType.DMA((cols // 2,)),
            pltpu.SemaphoreType.DMA((cols // 2,)),
            pltpu.SemaphoreType.DMA((cols // 2,)),
            pltpu.SemaphoreType.DMA((cols // 2,)),
        ],
        compiler_params=pltpu.CompilerParams(collective_id=0, has_side_effects=True),
    )(
        short_taps.reshape(9, width),
        skip,
        decay_rate,
        tokens,
        w_value,
        w_gate_one,
        w_gate_two,
        w_out,
        params,
        *tables,
    )


EARLY = 6


def solution(mesh):
    placed = (
        P("row", None),
        P("col", None),
        P("col", None),
        P("col", None),
        P(None, None, "col"),
        P(),
        P(),
        P(),
        P("col"),
        P(None, "col"),
        P(None, "col"),
    )
    return jax.shard_map(
        on_device, mesh=mesh, in_specs=placed, out_specs=P("row", "col"), check_vma=False
    )
```

time: 116 us -> 58.1 us (0.50)
  Pallas kernels: 0 us -> 50.4 us
  blocking collectives: 44.5 us -> 0 us
  matrix products: 40.8 us -> 0 us
  starting transfers between devices: 18.8 us -> 0 us
  local copies, waits for them, and re-layouts: 8.61 us -> 5.77 us
    pallas_call x0 -> x1, Pallas kernels: none -> 50.4 us  [on_device(): pl.pallas_call(functools.partial(kernel, (rows, cols, chan, early)), out_...]
    dot_general x37 -> x0, matrix products: 40.8 us -> none  [the longest x1 7.98 us: filter_bank(): hidden = jnp.sin(jnp.dot(feats, filter_in, precision=HIGHEST))]
    all_to_all x1 -> x0, blocking collectives: 22.8 us -> none  [on_device(): lax.all_to_all(mixer_channels, 'row', split_axis=1, concat_axis=0, tiled=...]
    all_gather x1 -> x0, blocking collectives: 21.7 us -> none  [on_device(): lax.all_gather(position_major, 'col', axis=0, tiled=True)]
    all_to_all x1 -> x0, starting transfers between devices: 18.8 us -> none  [on_device(): lax.all_to_all(projected, 'row', split_axis=1, concat_axis=2, tiled=True)]
    unnamed x23 -> x5, local copies, waits for them, and re-layouts: 5.67 us -> 3.14 us
    cos x1 -> x0, other arithmetic: 1.44 us -> none  [filter_bank(): jnp.cos(angles)]
  transfers between devices with their start and end apart: 1 -> 0, of which waited for: 0 -> 0; matrix products, arithmetic and copies ran while one was open for 28% -> 0% of each run, Pallas kernels for 0% -> 0%
where the time goes in v1:
time: 58.1 us; the launch traced here: 57.7 us
  Pallas kernels  50.4 us (87%)
  local copies, waits for them, and re-layouts  5.77 us (10%)
  other arithmetic  1.44 us (2%)
    pallas_call x1, Pallas kernels, on_device(): pl.pallas_call(functools.partial(kernel, (rows, cols, chan, early)), out_...  50.4 us
    unnamed x5, local copies, waits for them, and re-layouts  3.14 us
    slice x2, local copies, waits for them, and re-layouts, on_device(): first_w = jnp.concatenate([filter_in[1:], filter_in[:1]]).T * turns  1.42 us

profile of v1, /device:TPU:1, one launch (start us, length us, event | category | flops | bytes accessed | tf_op | source)
XLA Modules:
  0.0 57.7 jit_solution(12191007912425311434)
XLA Ops:
  0.0 0.0 copy-start
  0.0 0.0 copy-start.1
  0.0 1.7 %copy-done = f32[64,2,2,2304]{3,2,1,0:T(2,128)S(1)} copy-done((f32[64,2,2,2304]{3,2,1,0:T(2,128)S(1)}, f32[64,2,2,2304]{3,2,1,0:T(2,128)}, u32[]{:S(2)}) %copy-start) | copy-done | bytes 2359320
  1.7 0.2 constant_dynamic-slice_fusion
  1.9 0.1 copy.22
  2.0 0.1 tile.32
  2.1 0.7 %slice.6 = f32[32,64]{1,0:T(8,128)S(1)} slice(f32[33,64]{1,0:T(8,128)} %param.22), slice={[1:33], [0:64]} | slice | bytes 16384 | tf_op jit(solution)/shard_map/slice | solution.py:423
  2.8 0.7 %slice.7 = f32[1,64]{1,0:T(1,128)S(1)} slice(f32[33,64]{1,0:T(8,128)} %param.22), slice={[0:1], [0:64]} | slice | bytes 512 | tf_op jit(solution)/shard_map/slice | solution.py:423
  3.6 0.1 copy.20
  3.6 0.8 %multiply_bitcast_fusion = f32[64,64]{0,1:T(8,128)S(1)} fusion(f32[64,64]{1,0:T(8,128)} %param.23), kind=kLoop, calls=%fused_computation.7 | loop fusion | flops 4096 | bytes 32768 | tf_op jit(solution)/shard_map/mul | solution.py:429
  4.4 0.1 copy.21
  4.5 0.7 %select_maximum_fusion.params = f32[144,256]{1,0:T(8,128)} fusion(f32[16,192]{1,0:T(8,128)S(1)} %tile.32, f32[64,192]{1,0:T(8,128)S(1)} %copy.21, f32[64,144]{1,0:T(8,128)S(1)} %copy.20), kind=kLoop, calls=%fused_computation.2 | loop fusion | flops 368640 | bytes 245760 | tf_op jit(solution)/shard_map/concatenate | solution.py:426
  5.2 0.0 copy-done.1
  5.2 0.6 %reshape.18.taps_s = f32[9,144]{1,0:T(8,128)} reshape(f32[3,3,144]{2,1,0:T(4,128)S(1)} %copy-done.1) | data formatting | bytes 10368 | tf_op jit(solution)/shard_map/reshape | solution.py:468
  5.8 50.4 %shard_map.163 = bf16[128,256]{1,0:T(8,128)(2,1)} custom-call(f32[9,144]{1,0:T(8,128)} %reshape.18.taps_s, f32[2,144]{1,0:T(2,128)} %skip_s.1, f32[144]{0:T(256)} %rate_s.1, bf16[128,4096]{1,0:T(8,128)(2,1)} %tokens_h.1, bf16[144,4096]{1,0:T(8,128)(2,1)} %value_h.1, bf16[144,4096]{1,0:T(8,128)(2,1)} %gate_one_h.1, bf16[144,4096]{1,0:T(8,128)(2,1)} %gate_two_h.1, ...), custom_call_target="tpu_custom_call" | custom-call | tf_op jit(solution)/shard_map/pallas_call | solution.py:438
  56.2 1.5 %copy.24 = bf16[128,256]{1,0:T(8,128)(2,1)} copy(bf16[128,256]{1,0:T(8,128)(2,1)} %shard_map.163) | data formatting | bytes 131072
  (7 shorter events, 0.1 us)
Async XLA Ops:
  0.0 1.7 %copy-start = (f32[64,2,2,2304]{3,2,1,0:T(2,128)S(1)}, f32[64,2,2,2304]{3,2,1,0:T(2,128)}, u32[]{:S(2)}) copy-start(f32[64,2,2,2304]{3,2,1,0:T(2,128)} %param.24) | copy-start | bytes 7077892
  0.0 5.2 %copy-start.1 = (f32[3,3,144]{2,1,0:T(4,128)S(1)}, f32[3,3,144]{2,1,0:T(4,128)}, u32[]{:S(2)}) copy-start(f32[3,3,144]{2,1,0:T(4,128)} %param.21) | copy-start | bytes 15556

commit v2 on v1

v2 whole, which is shorter than its diff:
```python
import functools
import math

import jax
import jax.numpy as jnp
import ml_dtypes
import numpy as np
from jax import lax
from jax.experimental import pallas as pl
from jax.experimental.pallas import tpu as pltpu
from jax.sharding import PartitionSpec as P

BANDS = 16
BLOCK = 128
CHUNK_BLOCKS = 16
SINE = (
    6.283182818553798,
    -41.341421398897,
    81.59618387742557,
    -76.58010056369793,
    41.20539500742814,
    -12.271262547422271,
)
ROUNDER = 12582912.0
PARCELS = (((0, 0), (0, 1), (0, 2), (1, 0)), ((1, 1), (1, 2), (2, 0), (2, 1)), ((2, 2), None))
MESH = pl.DeviceIdType.MESH
F32 = jnp.float32
BF16 = jnp.bfloat16


def halves(table):
    high = table.astype(ml_dtypes.bfloat16)
    low = (table - high.astype(np.float64)).astype(ml_dtypes.bfloat16)
    return high, low


def constants(rows, seq_len):
    wide = 2 * rows
    total = wide * BLOCK
    odd = np.arange(rows)[:, None] + 0.5
    blocks = np.arange(rows)[None, :]
    one = 2 * np.pi * odd * blocks / wide
    first = np.concatenate([np.cos(one), -np.sin(one)], axis=0)
    last = np.concatenate([np.cos(one).T, -np.sin(one).T], axis=1) * (2.0 / total)
    first_h, first_l = halves(first)
    last_h, last_l = halves(last)
    first = np.concatenate([first_h, first_l, first_h], axis=1)
    last = np.concatenate([last_h, last_l, last_h], axis=1)
    lanes = np.arange(BLOCK)
    two = 2 * np.pi * odd * lanes[None, :] / total
    twiddle = np.stack([np.cos(two), np.sin(two)]).astype(np.float32)
    three = 2 * np.pi * (lanes[:, None] * lanes[None, :] % BLOCK) / BLOCK
    cosine, sine = np.cos(three), np.sin(three)
    forward = np.block([[cosine, -sine], [sine, cosine]])
    inverse = np.block([[cosine, sine], [-sine, cosine]])
    square = np.stack([*halves(forward), *halves(inverse)])
    chunk = CHUNK_BLOCKS * BLOCK
    bands = np.linspace(0.0001, BANDS - 1, BANDS, dtype=np.float32).astype(np.float64)
    rate = 2 * np.pi / seq_len * bands[:, None]
    inside = rate * np.arange(chunk)[None, :]
    base = np.concatenate([np.cos(inside), np.sin(inside)]).astype(np.float32)
    steps = np.arange(seq_len // chunk)[:, None, None] * chunk * rate[None]
    turn = np.concatenate([np.cos(steps), np.sin(steps)], axis=1)
    turn = np.broadcast_to(turn, turn.shape[:2] + (BLOCK,)).astype(np.float32)
    return first, last, twiddle, square, base, np.ascontiguousarray(turn)


def timed(name, wait):
    with jax.named_scope(name):
        wait()


def dot(left, right, dims=((1,), (0,))):
    return lax.dot_general(left, right, (dims, ((), ())), preferred_element_type=F32)


def split(value):
    high = value.astype(BF16)
    return high, (value - high.astype(F32)).astype(BF16)


def sine_of_turns(turns):
    part = turns - ((turns + ROUNDER) - ROUNDER)
    square = part * part
    total = jnp.full_like(square, SINE[-1])
    for coefficient in SINE[-2::-1]:
        total = total * square + coefficient
    return total * part


def stacked(value):
    high, low = split(value)
    return jnp.concatenate([high, high, low], axis=0)


def tripled(weights, width):
    high = weights.astype(BF16).astype(F32)
    lane = lax.broadcasted_iota(jnp.int32, weights.shape, 1)
    middle = (lane >= width) & (lane < 2 * width)
    return jnp.where(middle, weights - high, high).astype(BF16)


def kernel(
    sizes,
    taps_h,
    skip_h,
    rate_h,
    tokens_h,
    value_h,
    gate_one_h,
    gate_two_h,
    out_h,
    filter_in_h,
    filter_mid_h,
    filter_out_h,
    first_h,
    last_h,
    twiddle_h,
    square_h,
    base_h,
    turn_h,
    result,
    taps_s,
    skip_s,
    rate_s,
    filter_in,
    filter_mid,
    filter_out,
    first,
    last,
    twiddle,
    square,
    base,
    turn,
    flip,
    tokens_v,
    weights_v,
    out_v,
    plain,
    spread,
    gathered_taps,
    spectra,
    send_a,
    send_b,
    send_c,
    recv_a,
    recv_b,
    recv_c,
    send_y,
    recv_y,
    blocks,
    load_sem,
    send_sem,
    recv_sem,
    near_send,
    near_recv,
    pair_send,
    pair_recv,
):
    rows, cols, chan = sizes
    width = rows * chan
    chips = cols // 2
    row = lax.axis_index("row")
    col = lax.axis_index("col")
    place = col // 2
    core = col % 2
    partner = place * 2 + 1 - core

    own = col * width + row * chan
    window = jnp.minimum(own // 128, filter_out_h.shape[3] // 128 - 2) * 128
    window = pl.multiple_of(window, 128)
    pairs = [
        (tokens_h, tokens_v),
        (value_h, weights_v.at[0]),
        (gate_one_h, weights_v.at[1]),
        (gate_two_h, weights_v.at[2]),
        (filter_in_h, filter_in),
        (filter_mid_h, filter_mid),
        (filter_out_h.at[:, :, :, pl.ds(window, 256)], filter_out),
        (base_h, base),
        (turn_h, turn),
        (first_h, first),
        (last_h, last),
        (twiddle_h, twiddle),
        (square_h, square),
        (out_h, out_v),
        (rate_h, rate_s),
        (taps_h, taps_s),
        (skip_h, skip_s),
    ]
    loads = [pltpu.make_async_copy(*pair, load_sem.at[at]) for at, pair in enumerate(pairs)]
    for load in loads[:2]:
        load.start()

    barrier = pltpu.get_barrier_semaphore()

    def wrapped(index, extent):
        return jnp.where(index >= extent, index - extent, index)

    def far_first(visit):
        middle = rows // 2
        visit(wrapped(row + middle, rows))

        @pl.loop(1, middle)
        def _(step):
            visit(wrapped(row + middle + step, rows))
            visit(wrapped(row + middle - step, rows))

    def greet(other):
        pl.semaphore_signal(barrier, inc=1, device_id=(other, col), device_id_type=MESH)

    far_first(greet)
    for step in range(1, chips):
        other = wrapped(place + step, chips) * 2 + core
        pl.semaphore_signal(barrier, inc=1, device_id=(row, other), device_id_type=MESH)
    pl.semaphore_signal(barrier, inc=1, device_id=(row, partner), device_id_type=MESH)
    for load in loads[2:]:
        load.start()

    def send(source, landing, which):
        def visit(other):
            pltpu.make_async_remote_copy(
                src_ref=source.at[other],
                dst_ref=landing.at[row],
                send_sem=send_sem.at[which],
                recv_sem=recv_sem.at[which],
                device_id=(other, col),
                device_id_type=MESH,
            ).start()

        far_first(visit)

    def all_of(source, landing, which):
        return pltpu.make_async_remote_copy(
            src_ref=source.at[pl.ds(0, rows - 1)],
            dst_ref=landing.at[pl.ds(0, rows - 1)],
            send_sem=send_sem.at[which],
            recv_sem=recv_sem.at[which],
            device_id=(wrapped(row + 1, rows), col),
            device_id_type=MESH,
        )

    outgoing = (send_a, send_b, send_c)
    incoming = (recv_a, recv_b, recv_c)

    timed("load_tokens", loads[0].wait)
    for which in range(3):
        timed("load_weights", loads[1 + which].wait)
        projected = dot(weights_v[which], tokens_v[...], ((1,), (1,)))
        plain[...] = projected.astype(BF16).astype(F32)
        for parcel, members in enumerate(PARCELS):
            for slot, member in enumerate(members):
                if member is not None and member[0] == which:
                    spread[parcel, pl.ds(slot, rows, stride=len(members)), :] = plain[
                        pl.ds(member[1], rows, stride=chan), :
                    ]
    spread[2, pl.ds(1, rows, stride=2), :] = jnp.zeros((rows, BLOCK), F32)
    for parcel, members in enumerate(PARCELS):
        size = len(members)
        for r in range(rows):
            outgoing[parcel][r] = spread[parcel, size * r : size * r + size, :].astype(BF16)

    n_chunks = rows // CHUNK_BLOCKS
    chunk = CHUNK_BLOCKS * BLOCK
    seq_len = rows * BLOCK
    for load in loads[4:9] + loads[14:15]:
        timed("load_filter", load.wait)
    turns = 1 / (2 * math.pi)
    flip[...] = jnp.zeros_like(flip)
    for copy in range(3):
        flip[48 * copy : 48 * copy + 32, 0:64] = filter_in[1:33, :] * turns
        flip[48 * copy + 32 : 48 * copy + 33, 0:64] = filter_in[0:1, :] * turns
    in_w = tripled(flip[...].T[0:64, 0:144], 48)
    for copy in range(3):
        flip[64 * copy : 64 * copy + 64, 0:64] = filter_mid[...] * turns
    mid_w = tripled(flip[...].T[0:64, 0:192], 64)
    pick_row = lax.broadcasted_iota(jnp.int32, (16, 256), 0)
    pick_lane = lax.broadcasted_iota(jnp.int32, (16, 256), 1)
    out_w = jnp.zeros((16, 192), F32)
    for kind in range(4):
        high, low = split(filter_out[:, kind // 2, kind % 2, :])
        wanted = (pick_row // chan == kind) & (pick_lane == own - window + pick_row % chan)
        pick = jnp.where(wanted, 1.0, 0.0).astype(BF16)
        out_w += dot(pick, jnp.concatenate([high, low, high], axis=0), ((1,), (1,)))
    out_w = out_w.astype(BF16)
    rate_rows = jnp.zeros((16, BLOCK), F32)
    channel = lax.rem(lax.broadcasted_iota(jnp.int32, (16, BLOCK), 0), chan)
    for q in range(chan):
        rate_rows = jnp.where(channel == q, rate_s[row * chan + q], rate_rows)
    rate_rows = jnp.concatenate([rate_rows] * CHUNK_BLOCKS, axis=1)

    def filter_chunk(index):
        lane = lax.broadcasted_iota(jnp.int32, (16, chunk), 1)
        relative = (lane + index * chunk).astype(F32) * (1.0 / (seq_len - 1))
        first_row = lax.broadcasted_iota(jnp.int32, (16, chunk), 0) == 0
        turn_c = jnp.concatenate([turn[index, 0:BANDS, :]] * CHUNK_BLOCKS, axis=1)
        turn_s = jnp.concatenate([turn[index, BANDS : 2 * BANDS, :]] * CHUNK_BLOCKS, axis=1)
        base_c, base_s = base[0:BANDS, :], base[BANDS : 2 * BANDS, :]
        feats = jnp.concatenate(
            [
                base_c * turn_c - base_s * turn_s,
                base_s * turn_c + base_c * turn_s,
                jnp.where(first_row, relative, 0.0),
            ],
            axis=0,
        )
        hidden = sine_of_turns(dot(in_w, stacked(feats)))
        hidden = sine_of_turns(dot(mid_w, stacked(hidden)))
        filter_taps = dot(out_w, stacked(hidden)) * jnp.exp(-relative * rate_rows)
        for b in range(CHUNK_BLOCKS):
            start = pl.multiple_of((index * CHUNK_BLOCKS + b) * 16, 16)
            gathered_taps[pl.ds(start, 16), :] = filter_taps[:, b * BLOCK : (b + 1) * BLOCK]

    timed("barrier", lambda: pl.semaphore_wait(barrier, rows - 1 + chips - 1 + 1))
    for parcel in range(3):
        send(outgoing[parcel], incoming[parcel], parcel)
    for parcel in range(3):
        incoming[parcel][row] = outgoing[parcel][row]

    @pl.loop(0, n_chunks)
    def _(index):
        filter_chunk(index)

    for load in loads[9:13] + loads[15:17]:
        timed("load_tables", load.wait)
    tw_c, tw_s = twiddle[0], twiddle[1]

    def forward(signals):
        reals, imags = [], []
        for signal in signals:
            both = dot(first[...], stacked(signal))
            re, im = both[:rows], both[rows:]
            reals.append(re * tw_c + im * tw_s)
            imags.append(im * tw_c - re * tw_s)
        both = jnp.concatenate(
            [jnp.concatenate(reals, axis=0), jnp.concatenate(imags, axis=0)], axis=1
        )
        high, low = split(both)
        return dot(high, square[0]) + dot(high, square[1]) + dot(low, square[0])

    def backward(spectrum):
        high, low = split(spectrum)
        both = dot(high, square[2]) + dot(high, square[3]) + dot(low, square[2])
        signals = []
        for q in range(chan):
            re = both[q * rows : (q + 1) * rows, :BLOCK]
            im = both[q * rows : (q + 1) * rows, BLOCK:]
            turned = jnp.concatenate([re * tw_c - im * tw_s, im * tw_c + re * tw_s], axis=0)
            signals.append(dot(last[...], stacked(turned)))
        return signals

    lane = lax.broadcasted_iota(jnp.int32, (rows, BLOCK), 1)
    line = lax.broadcasted_iota(jnp.int32, (rows, BLOCK), 0)
    origin = (lane == 0) & (line == 0)
    for order in range(2):
        ahead, behind = [], []
        for q in range(chan):
            base_row = (order * 2) * chan + q
            ahead.append(gathered_taps[pl.ds(base_row, rows, stride=16), :])
            back = gathered_taps[pl.ds(base_row + chan, rows, stride=16), :]
            behind.append(jnp.where(origin, 0.0, back))
        ahead = forward(ahead)
        behind = forward(behind)
        spectra[order, :, :BLOCK] = ahead[:, :BLOCK] + behind[:, :BLOCK]
        spectra[order, :, BLOCK:] = ahead[:, BLOCK:] - behind[:, BLOCK:]

    def short(signal, which, q):
        before = pltpu.roll(signal, 1, 1)
        before = jnp.where(lane == 0, pltpu.roll(before, 1, 0), before)
        before = jnp.where(origin, 0.0, before)
        after = pltpu.roll(signal, BLOCK - 1, 1)
        after = jnp.where(lane == BLOCK - 1, pltpu.roll(after, rows - 1, 0), after)
        after = jnp.where((lane == BLOCK - 1) & (line == rows - 1), 0.0, after)
        at = row * chan + q
        return (
            before * taps_s[which, 0, at]
            + signal * taps_s[which, 1, at]
            + after * taps_s[which, 2, at]
        )

    def unpack(parcel):
        wait = all_of(outgoing[parcel], incoming[parcel], parcel).wait_recv
        timed(f"parcel_{parcel}_in", wait)
        size = len(PARCELS[parcel])
        for r in range(rows):
            spread[parcel, size * r : size * r + size, :] = incoming[parcel][r].astype(F32)

    def shorted(which):
        found = []
        for q in range(chan):
            for parcel, members in enumerate(PARCELS):
                if (which, q) in members:
                    rows_of = pl.ds(members.index((which, q)), rows, stride=len(members))
                    found.append(short(spread[parcel, rows_of, :], which, q))
        return found

    unpack(0)
    signals = shorted(0)
    for order in range(2):
        spectrum = forward(signals)
        re, im = spectrum[:, :BLOCK], spectrum[:, BLOCK:]
        kern_re, kern_im = spectra[order, :, :BLOCK], spectra[order, :, BLOCK:]
        product = jnp.concatenate(
            [re * kern_re - im * kern_im, re * kern_im + im * kern_re], axis=1
        )
        longs = backward(product)
        unpack(1 + order)
        gates = shorted(1 + order)
        for q in range(chan):
            signals[q] = gates[q] * (longs[q] + skip_s[order, row * chan + q] * signals[q])

    for q in range(4):
        spread[0, pl.ds(q, rows, stride=4), :] = (
            signals[q] if q < chan else jnp.zeros((rows, BLOCK), F32)
        )
    for r in range(rows):
        send_y[r] = spread[0, 4 * r : 4 * r + 4, :].astype(BF16)
    send(send_y, recv_y, 3)
    recv_y[row] = send_y[row]
    timed("mixer_in", all_of(send_y, recv_y, 3).wait_recv)
    for r in range(rows):
        spread[0, 4 * r : 4 * r + 4, :] = recv_y[r].astype(F32)
    for q in range(chan):
        plain[pl.ds(q, rows, stride=chan), :] = spread[0, pl.ds(q, rows, stride=4), :]
    blocks[col] = plain[...].astype(BF16)

    def to_chip(step):
        return pltpu.make_async_remote_copy(
            src_ref=blocks.at[col],
            dst_ref=blocks.at[col],
            send_sem=near_send.at[step],
            recv_sem=near_recv.at[step],
            device_id=(row, wrapped(place + step, chips) * 2 + core),
            device_id_type=MESH,
        )

    def source(step):
        return wrapped(place + chips - step, chips)

    def to_pair(step):
        own = source(step) * 2 + core
        return pltpu.make_async_remote_copy(
            src_ref=blocks.at[own],
            dst_ref=blocks.at[own],
            send_sem=pair_send.at[step],
            recv_sem=pair_recv.at[step],
            device_id=(row, partner),
            device_id_type=MESH,
        )

    def product(indices):
        left = jnp.concatenate([blocks[index] for index in indices], axis=0)
        starts = [pl.multiple_of(index * width, 16) for index in indices]
        right = jnp.concatenate([out_v[pl.ds(start, width), :] for start in starts], axis=0)
        return dot(left, right, ((0,), (0,)))

    half = chips // 2
    before = jnp.where(core == 0, half - 1, half + 1)
    after = chips - before
    hand = wrapped(place + chips - before, chips) * 2 + core
    onward = wrapped(place + chips - 1 + 2 * (1 - core), 2 * chips)
    onward = wrapped(onward, chips)

    relay = pltpu.make_async_remote_copy(
        src_ref=blocks.at[hand],
        dst_ref=blocks.at[hand],
        send_sem=near_send.at[half],
        recv_sem=near_recv.at[half],
        device_id=(row, onward * 2 + core),
        device_id_type=MESH,
    )
    steps = [before, after] + [s for d in range(half - 2, 0, -1) for s in (d, chips - d)]
    for step in steps:
        to_chip(step).start()
    to_pair(0).start()
    timed("load_out", loads[13].wait)
    steps.insert(-2, half)
    middle = 3
    total = jnp.zeros((BLOCK, out_v.shape[1]), F32)
    for at, step in enumerate(steps):
        timed("near_in", to_chip(step).wait_recv)
        if at == 0:
            relay.start()
        to_pair(step).start()
        if at == middle:
            total += product([source(s) * 2 + core for s in [0] + steps[: middle + 1]])
    total += product([source(s) * 2 + core for s in steps[middle + 1 :]])
    for group in ([0] + steps[:middle], steps[middle:]):
        for step in group:
            timed("pair_in", to_pair(step).wait_recv)
        total += product([source(step) * 2 + 1 - core for step in group])
    result[...] = total.astype(BF16)

    for parcel in range(3):
        all_of(outgoing[parcel], incoming[parcel], parcel).wait_send()
    timed("drain", all_of(send_y, recv_y, 3).wait_send)
    for step in steps:
        to_chip(step).wait_send()
    for step in [0] + steps:
        to_pair(step).wait_send()


def on_device(
    tokens,
    w_value,
    w_gate_one,
    w_gate_two,
    short_taps,
    filter_in,
    filter_mid,
    filter_out,
    decay_rate,
    skip,
    w_out,
):
    rows, cols = lax.axis_size("row"), lax.axis_size("col")
    width, depth = w_value.shape
    chan = width // rows
    seq_len = rows * BLOCK
    tables = [jnp.asarray(table) for table in constants(rows, seq_len)]
    vmem = pl.BlockSpec(memory_space=pltpu.VMEM)
    hbm = pl.BlockSpec(memory_space=pl.ANY)
    return pl.pallas_call(
        functools.partial(kernel, (rows, cols, chan)),
        out_shape=pltpu.VMEM((BLOCK, w_out.shape[1]), BF16),
        in_specs=[hbm] * 17,
        out_specs=vmem,
        scratch_shapes=[
            pltpu.SMEM(short_taps.shape, F32),
            pltpu.SMEM(skip.shape, F32),
            pltpu.SMEM(decay_rate.shape, F32),
            pltpu.VMEM(filter_in.shape, F32),
            pltpu.VMEM(filter_mid.shape, F32),
            pltpu.VMEM(filter_out.shape[:3] + (256,), F32),
            *[pltpu.VMEM(table.shape, table.dtype) for table in tables],
            pltpu.VMEM((256, 128), F32),
            pltpu.VMEM((BLOCK, depth), BF16),
            pltpu.VMEM((3, width, depth), BF16),
            pltpu.VMEM(w_out.shape, BF16),
            pltpu.VMEM((width, BLOCK), F32),
            pltpu.VMEM((3, 4 * rows, BLOCK), F32),
            pltpu.VMEM((16 * rows, BLOCK), F32),
            pltpu.VMEM((2, width, 2 * BLOCK), F32),
            *[pltpu.VMEM((rows, len(members), BLOCK), BF16) for members in PARCELS],
            *[pltpu.VMEM((rows, len(members), BLOCK), BF16) for members in PARCELS],
            pltpu.VMEM((rows, 4, BLOCK), BF16),
            pltpu.VMEM((rows, 4, BLOCK), BF16),
            pltpu.VMEM((cols, width, BLOCK), BF16),
            pltpu.SemaphoreType.DMA((17,)),
            pltpu.SemaphoreType.DMA((4,)),
            pltpu.SemaphoreType.DMA((4,)),
            pltpu.SemaphoreType.DMA((cols // 2,)),
            pltpu.SemaphoreType.DMA((cols // 2,)),
            pltpu.SemaphoreType.DMA((cols // 2,)),
            pltpu.SemaphoreType.DMA((cols // 2,)),
        ],
        compiler_params=pltpu.CompilerParams(collective_id=0, has_side_effects=True),
    )(
        short_taps,
        skip,
        decay_rate,
        tokens,
        w_value,
        w_gate_one,
        w_gate_two,
        w_out,
        filter_in,
        filter_mid,
        filter_out,
        *tables,
    )


def solution(mesh):
    placed = (
        P("row", None),
        P("col", None),
        P("col", None),
        P("col", None),
        P(None, None, "col"),
        P(),
        P(),
        P(),
        P("col"),
        P(None, "col"),
        P(None, "col"),
    )
    return jax.shard_map(
        on_device, mesh=mesh, in_specs=placed, out_specs=P("row", "col"), check_vma=False
    )
```

time: 58.1 us -> 48.4 us (0.83)
  local copies, waits for them, and re-layouts: 5.77 us -> 0.63 us
  Pallas kernels: 50.4 us -> 47.7 us
  other arithmetic: 1.44 us -> 0 us
    pallas_call x1, Pallas kernels: 50.4 us -> 47.7 us  [on_device(): pl.pallas_call(functools.partial(kernel, (rows, cols, chan)), out_shape=p...]
    unnamed x5 -> x1, local copies, waits for them, and re-layouts: 3.14 us -> 0.63 us
    slice x2 -> x0, local copies, waits for them, and re-layouts: 1.42 us -> none  [on_device(): first_w = jnp.concatenate([filter_in[1:], filter_in[:1]]).T * turns]
    mul x2 -> x0, other arithmetic: 0.77 us -> none  [the longest x1 0.76 us: on_device(): filter_mid.T * turns]
    concatenate x1 -> x0, other arithmetic: 0.66 us -> none  [on_device(): jnp.concatenate([jnp.pad(jnp.tile(first_w, (1, 3)), ((0, 0), (0, 112))),...]
    reshape x2 -> x0, local copies, waits for them, and re-layouts: 0.63 us -> none  [the longest x1 0.61 us: on_device(): short_taps.reshape(9, width)]
where the time goes in v2:
time: 48.4 us; the launch traced here: 48.3 us
  Pallas kernels  47.7 us (99%)
  local copies, waits for them, and re-layouts  0.63 us (1%)
    pallas_call x1, Pallas kernels, on_device(): pl.pallas_call(functools.partial(kernel, (rows, cols, chan)), out_shape=p...  47.7 us

profile of v2, /device:TPU:1, one launch (start us, length us, event | category | flops | bytes accessed | tf_op | source)
XLA Modules:
  0.0 48.3 jit_solution(3670140532298142465)
XLA Ops:
  0.0 47.7 %shard_map.163 = bf16[128,256]{1,0:T(8,128)(2,1)S(1)} custom-call(f32[3,3,144]{2,1,0:T(4,128)} %taps_h.1, f32[2,144]{1,0:T(2,128)} %skip_h.1, f32[144]{0:T(256)} %rate_h.1, bf16[128,4096]{1,0:T(8,128)(2,1)} %tokens_h.1, bf16[144,4096]{1,0:T(8,128)(2,1)} %value_h.1, bf16[144,4096]{1,0:T(8,128)(2,1)} %gate_one_h.1, bf16[144,4096]{1,0:T(8,128)(2,1)} %gate_two_h.1, ...), custom_call_target="tpu_custom_call" | custom-call | tf_op jit(solution)/shard_map/pallas_call | solution.py:523
  47.7 0.6 %copy.19 = bf16[128,256]{1,0:T(8,128)(2,1)} copy(bf16[128,256]{1,0:T(8,128)(2,1)S(1)} %shard_map.163) | data formatting | bytes 131072

commit v3 on v2

--- a/solution.py
+++ b/solution.py
@@ -22,6 +22,7 @@
     -12.271262547422271,
 )
 ROUNDER = 12582912.0
+GROUPS = 3
 PARCELS = (((0, 0), (0, 1), (0, 2), (1, 0)), ((1, 1), (1, 2), (2, 0), (2, 1)), ((2, 2), None))
 MESH = pl.DeviceIdType.MESH
 F32 = jnp.float32
@@ -217,13 +218,13 @@
     for load in loads[2:]:
         load.start()
 
-    def send(source, landing, which):
+    def send(source, landing, which, landed):
         def visit(other):
             pltpu.make_async_remote_copy(
                 src_ref=source.at[other],
                 dst_ref=landing.at[row],
                 send_sem=send_sem.at[which],
-                recv_sem=recv_sem.at[which],
+                recv_sem=recv_sem.at[landed],
                 device_id=(other, col),
                 device_id_type=MESH,
             ).start()
@@ -313,7 +314,7 @@
 
     timed("barrier", lambda: pl.semaphore_wait(barrier, rows - 1 + chips - 1 + 1))
     for parcel in range(3):
-        send(outgoing[parcel], incoming[parcel], parcel)
+        send(outgoing[parcel], incoming[parcel], parcel, parcel)
     for parcel in range(3):
         incoming[parcel][row] = outgoing[parcel][row]
 
@@ -415,89 +416,98 @@
         )
     for r in range(rows):
         send_y[r] = spread[0, 4 * r : 4 * r + 4, :].astype(BF16)
-    send(send_y, recv_y, 3)
+    near = rows // GROUPS
+    share = near * chan
+    mine = lax.div(row, near)
+    send(send_y, recv_y, 3, 3 + mine)
     recv_y[row] = send_y[row]
-    timed("mixer_in", all_of(send_y, recv_y, 3).wait_recv)
-    for r in range(rows):
-        spread[0, 4 * r : 4 * r + 4, :] = recv_y[r].astype(F32)
-    for q in range(chan):
-        plain[pl.ds(q, rows, stride=chan), :] = spread[0, pl.ds(q, rows, stride=4), :]
-    blocks[col] = plain[...].astype(BF16)
-
-    def to_chip(step):
+
+    def source(step):
+        return wrapped(place + chips - step, chips)
+
+    lower = wrapped(mine + GROUPS - 1, GROUPS)
+    upper = wrapped(mine + 1, GROUPS)
+    low_half = row - mine * near < near // 2
+    groups = [mine, jnp.where(low_half, lower, upper), jnp.where(low_half, upper, lower)]
+
+    def to_chip(at, step):
         return pltpu.make_async_remote_copy(
-            src_ref=blocks.at[col],
-            dst_ref=blocks.at[col],
-            send_sem=near_send.at[step],
-            recv_sem=near_recv.at[step],
+            src_ref=blocks.at[col, groups[at]],
+            dst_ref=blocks.at[col, groups[at]],
+            send_sem=near_send,
+            recv_sem=near_recv.at[at, step],
             device_id=(row, wrapped(place + step, chips) * 2 + core),
             device_id_type=MESH,
         )
 
-    def source(step):
-        return wrapped(place + chips - step, chips)
-
-    def to_pair(step):
+    def to_pair(at, step):
         own = source(step) * 2 + core
         return pltpu.make_async_remote_copy(
-            src_ref=blocks.at[own],
-            dst_ref=blocks.at[own],
-            send_sem=pair_send.at[step],
-            recv_sem=pair_recv.at[step],
+            src_ref=blocks.at[own, groups[at]],
+            dst_ref=blocks.at[own, groups[at]],
+            send_sem=pair_send,
+            recv_sem=pair_recv.at[at, step],
             device_id=(row, partner),
             device_id_type=MESH,
         )
 
-    def product(indices):
-        left = jnp.concatenate([blocks[index] for index in indices], axis=0)
-        starts = [pl.multiple_of(index * width, 16) for index in indices]
-        right = jnp.concatenate([out_v[pl.ds(start, width), :] for start in starts], axis=0)
+    def product(at, indices):
+        left = jnp.concatenate([blocks[index, groups[at]] for index in indices], axis=0)
+        starts = [pl.multiple_of(index * width + groups[at] * share, 16) for index in indices]
+        right = jnp.concatenate([out_v[pl.ds(start, share), :] for start in starts], axis=0)
         return dot(left, right, ((0,), (0,)))
 
-    half = chips // 2
-    before = jnp.where(core == 0, half - 1, half + 1)
-    after = chips - before
-    hand = wrapped(place + chips - before, chips) * 2 + core
-    onward = wrapped(place + chips - 1 + 2 * (1 - core), 2 * chips)
-    onward = wrapped(onward, chips)
-
-    relay = pltpu.make_async_remote_copy(
-        src_ref=blocks.at[hand],
-        dst_ref=blocks.at[hand],
-        send_sem=near_send.at[half],
-        recv_sem=near_recv.at[half],
-        device_id=(row, onward * 2 + core),
-        device_id_type=MESH,
-    )
-    steps = [before, after] + [s for d in range(half - 2, 0, -1) for s in (d, chips - d)]
-    for step in steps:
-        to_chip(step).start()
-    to_pair(0).start()
+    steps = [chips // 2] + [s for d in range(chips // 2 - 1, 0, -1) for s in (d, chips - d)]
+    for at in range(GROUPS):
+        arrivals = recv_y.at[pl.ds(0, near - 1 if at == 0 else near)]
+        group_in = pltpu.make_async_remote_copy(
+            src_ref=arrivals,
+            dst_ref=arrivals,
+            send_sem=send_sem.at[3],
+            recv_sem=recv_sem.at[3 + groups[at]],
+            device_id=(wrapped(row + 1, rows), col),
+            device_id_type=MESH,
+        )
+        timed(f"group_{at}_in", group_in.wait_recv)
+        for r in range(near):
+            spread[at, 4 * r : 4 * r + 4, :] = recv_y[groups[at] * near + r].astype(F32)
+        for q in range(chan):
+            plain[pl.ds(at * share + q, near, stride=chan), :] = spread[
+                at, pl.ds(q, near, stride=4), :
+            ]
+        blocks[col, groups[at]] = plain[at * share : (at + 1) * share, :].astype(BF16)
+        for step in steps:
+            to_chip(at, step).start()
+        to_pair(at, 0).start()
     timed("load_out", loads[13].wait)
-    steps.insert(-2, half)
-    middle = 3
-    total = jnp.zeros((BLOCK, out_v.shape[1]), F32)
-    for at, step in enumerate(steps):
-        timed("near_in", to_chip(step).wait_recv)
-        if at == 0:
-            relay.start()
-        to_pair(step).start()
-        if at == middle:
-            total += product([source(s) * 2 + core for s in [0] + steps[: middle + 1]])
-    total += product([source(s) * 2 + core for s in steps[middle + 1 :]])
-    for group in ([0] + steps[:middle], steps[middle:]):
-        for step in group:
-            timed("pair_in", to_pair(step).wait_recv)
-        total += product([source(step) * 2 + 1 - core for step in group])
-    result[...] = total.astype(BF16)
-
     for parcel in range(3):
         all_of(outgoing[parcel], incoming[parcel], parcel).wait_send()
     timed("drain", all_of(send_y, recv_y, 3).wait_send)
-    for step in steps:
-        to_chip(step).wait_send()
+    total = jnp.zeros((BLOCK, out_v.shape[1]), F32)
+    for at in range(GROUPS):
+        for step in steps:
+            timed("near_in", to_chip(at, step).wait_recv)
+            to_pair(at, step).start()
+        if at > 0:
+            for step in [0] + steps:
+                timed("pair_in", to_pair(at - 1, step).wait_recv)
+            total += product(at - 1, [source(step) * 2 + 1 - core for step in [0] + steps])
+        total += product(at, [source(step) * 2 + core for step in [0] + steps])
     for step in [0] + steps:
-        to_pair(step).wait_send()
+        timed("pair_in", to_pair(GROUPS - 1, step).wait_recv)
+    total += product(GROUPS - 1, [source(step) * 2 + 1 - core for step in [0] + steps])
+    result[...] = total.astype(BF16)
+
+    for sent, sem in ((steps, near_send), ([0] + steps, pair_send)):
+        sent = blocks.at[pl.ds(0, len(sent))]
+        pltpu.make_async_remote_copy(
+            src_ref=sent,
+            dst_ref=sent,
+            send_sem=sem,
+            recv_sem=recv_sem.at[0],
+            device_id=(row, partner),
+            device_id_type=MESH,
+        ).wait_send()
 
 
 def on_device(
@@ -545,14 +555,14 @@
             *[pltpu.VMEM((rows, len(members), BLOCK), BF16) for members in PARCELS],
             pltpu.VMEM((rows, 4, BLOCK), BF16),
             pltpu.VMEM((rows, 4, BLOCK), BF16),
-            pltpu.VMEM((cols, width, BLOCK), BF16),
+            pltpu.VMEM((cols, GROUPS, width // GROUPS, BLOCK), BF16),
             pltpu.SemaphoreType.DMA((17,)),
             pltpu.SemaphoreType.DMA((4,)),
-            pltpu.SemaphoreType.DMA((4,)),
-            pltpu.SemaphoreType.DMA((cols // 2,)),
-            pltpu.SemaphoreType.DMA((cols // 2,)),
-            pltpu.SemaphoreType.DMA((cols // 2,)),
-            pltpu.SemaphoreType.DMA((cols // 2,)),
+            pltpu.SemaphoreType.DMA((3 + GROUPS,)),
+            pltpu.SemaphoreType.DMA,
+            pltpu.SemaphoreType.DMA((GROUPS, cols // 2)),
+            pltpu.SemaphoreType.DMA,
+            pltpu.SemaphoreType.DMA((GROUPS, cols // 2)),
         ],
         compiler_params=pltpu.CompilerParams(collective_id=0, has_side_effects=True),
     )(

time: 48.4 us -> 46.3 us (0.957)
  Pallas kernels: 47.7 us -> 45.5 us
    pallas_call x1, Pallas kernels: 47.7 us -> 45.5 us  [on_device(): pl.pallas_call(functools.partial(kernel, (rows, cols, chan)), out_shape=p...]
where the time goes in v3:
time: 46.3 us; the launch traced here: 46.2 us
  Pallas kernels  45.5 us (98%)
  local copies, waits for them, and re-layouts  0.63 us (1%)
    pallas_call x1, Pallas kernels, on_device(): pl.pallas_call(functools.partial(kernel, (rows, cols, chan)), out_shape=p...  45.5 us

profile of v3, /device:TPU:1, one launch (start us, length us, event | category | flops | bytes accessed | tf_op | source)
XLA Modules:
  0.0 46.2 jit_solution(3124494819447319228)
XLA Ops:
  0.0 45.5 %shard_map.163 = bf16[128,256]{1,0:T(8,128)(2,1)S(1)} custom-call(f32[3,3,144]{2,1,0:T(4,128)} %taps_h.1, f32[2,144]{1,0:T(2,128)} %skip_h.1, f32[144]{0:T(256)} %rate_h.1, bf16[128,4096]{1,0:T(8,128)(2,1)} %tokens_h.1, bf16[144,4096]{1,0:T(8,128)(2,1)} %value_h.1, bf16[144,4096]{1,0:T(8,128)(2,1)} %gate_one_h.1, bf16[144,4096]{1,0:T(8,128)(2,1)} %gate_two_h.1, ...), custom_call_target="tpu_custom_call" | custom-call | tf_op jit(solution)/shard_map/pallas_call | solution.py:533
  45.6 0.6 %copy.19 = bf16[128,256]{1,0:T(8,128)(2,1)} copy(bf16[128,256]{1,0:T(8,128)(2,1)S(1)} %shard_map.163) | data formatting | bytes 131072

commit v4 on v3

--- a/solution.py
+++ b/solution.py
@@ -458,6 +458,7 @@
         return dot(left, right, ((0,), (0,)))
 
     steps = [chips // 2] + [s for d in range(chips // 2 - 1, 0, -1) for s in (d, chips - d)]
+    far, close = steps[:3], steps[3:]
     for at in range(GROUPS):
         arrivals = recv_y.at[pl.ds(0, near - 1 if at == 0 else near)]
         group_in = pltpu.make_async_remote_copy(
@@ -476,18 +477,28 @@
                 at, pl.ds(q, near, stride=4), :
             ]
         blocks[col, groups[at]] = plain[at * share : (at + 1) * share, :].astype(BF16)
-        for step in steps:
+        for step in far:
             to_chip(at, step).start()
         to_pair(at, 0).start()
+    for at in range(GROUPS):
+        for step in close:
+            to_chip(at, step).start()
     timed("load_out", loads[13].wait)
     for parcel in range(3):
         all_of(outgoing[parcel], incoming[parcel], parcel).wait_send()
     timed("drain", all_of(send_y, recv_y, 3).wait_send)
     total = jnp.zeros((BLOCK, out_v.shape[1]), F32)
-    for at in range(GROUPS):
-        for step in steps:
+    def pass_on(at, some):
+        for step in some:
             timed("near_in", to_chip(at, step).wait_recv)
             to_pair(at, step).start()
+
+    for at in range(GROUPS - 1):
+        pass_on(at, far[1:] + far[:1])
+    for at in range(GROUPS):
+        if at == GROUPS - 1:
+            pass_on(at, far[1:] + far[:1])
+        pass_on(at, close)
         if at > 0:
             for step in [0] + steps:
                 timed("pair_in", to_pair(at - 1, step).wait_recv)

time: 46.3 us -> 46.2 us (level)
  no operation moved by 1% of the time
where the time goes in v4:
time: 46.2 us; the launch traced here: 46 us
  Pallas kernels  45.4 us (98%)
  local copies, waits for them, and re-layouts  0.63 us (1%)
    pallas_call x1, Pallas kernels, on_device(): pl.pallas_call(functools.partial(kernel, (rows, cols, chan)), out_shape=p...  45.4 us

profile of v4, /device:TPU:1, one launch (start us, length us, event | category | flops | bytes accessed | tf_op | source)
XLA Modules:
  0.0 46.0 jit_solution(2436059647572882862)
XLA Ops:
  0.0 45.4 %shard_map.163 = bf16[128,256]{1,0:T(8,128)(2,1)S(1)} custom-call(f32[3,3,144]{2,1,0:T(4,128)} %taps_h.1, f32[2,144]{1,0:T(2,128)} %skip_h.1, f32[144]{0:T(256)} %rate_h.1, bf16[128,4096]{1,0:T(8,128)(2,1)} %tokens_h.1, bf16[144,4096]{1,0:T(8,128)(2,1)} %value_h.1, bf16[144,4096]{1,0:T(8,128)(2,1)} %gate_one_h.1, bf16[144,4096]{1,0:T(8,128)(2,1)} %gate_two_h.1, ...), custom_call_target="tpu_custom_call" | custom-call | tf_op jit(solution)/shard_map/pallas_call | solution.py:544
  45.4 0.6 %copy.19 = bf16[128,256]{1,0:T(8,128)(2,1)} copy(bf16[128,256]{1,0:T(8,128)(2,1)S(1)} %shard_map.163) | data formatting | bytes 131072
